TPU v7x, 512 devices: a whole 4x4x16 slice. The times are simulated.
512 devices in a mesh: ep: 32 (over z, core), tp: 16 (over y, x).
Axes of the slice: x: 4, y: 4, z: 16, core: 2. Of those that a mesh axis runs over, the one named last changes fastest.
Arguments:
- mixer_rows: bfloat16 [8192, 2048], P('ep'), may hold values from -8 to 8
- mixer_gain: float32 [2048], replicated, may hold values from 0.1 to 1.9
- w_query: bfloat16 [2048, 1024], P(None, 'tp'), may hold values from -0.125 to 0.125
- w_key: bfloat16 [2048, 1024], P(None, 'tp'), may hold values from -0.125 to 0.125
- w_value: bfloat16 [2048, 1024], P(None, 'tp'), may hold values from -0.125 to 0.125
- key_shift: float32 [16, 8192], P('tp'), may hold values from -14 to 0
- w_out: bfloat16 [1024, 2048], P(None, 'tp'), may hold values from -0.75 to 0.75
- expert_rows: bfloat16 [4096, 2048], P('ep'), may hold values from -6 to 6
- expert_gain: float32 [2048], replicated, may hold values from 0.1 to 1.9
- routes: int32 [4096, 4], P('ep'), may hold values from 0 to 31, all different within a row; in each aligned block of 128 rows (0 to 127, 128 to 255, ...) at most 32 rows name the same one
- route_weight: float32 [4096, 4], P('ep'), may hold values from 0.05 to 0.6
- w_gate: bfloat16 [32, 2048, 2048], P('ep', None, 'tp'), may hold values from -0.25 to 0.25
- w_up: bfloat16 [32, 2048, 2048], P('ep', None, 'tp'), may hold values from -0.25 to 0.25
- w_down: bfloat16 [32, 2048, 2048], P('ep', None, 'tp'), may hold values from -0.0625 to 0.0625
Outputs:
- mixer_out: bfloat16 [8192, 2048], P('ep', 'tp')
- expert_out: bfloat16 [4096, 2048], P('ep', 'tp')
Inputs may be any that keep to these rules, and one draw needn't show every extreme that they name: `routes`: each row names 4 different experts. In each aligned block of 128 rows no expert is named by more than 32 rows, and in every draw some block names some expert exactly 32 times.
All inputs are finite; a program needn't handle non-finite values.
Results may differ from a plain program's by a relative error of at most 0.0073.
Values may be sent and summed in bfloat16 or wider, within the bound.
A program may use at most 64 MiB of HBM per device.

v0:
```python
import jax
import jax.numpy as jnp
from jax import lax
from jax.sharding import Mesh
from jax.sharding import PartitionSpec as P

EP = ("ep_0", "ep_1")
norm_eps = 1e-06
glu_limit = 7.0
glu_alpha = 1.702


def in_order(blocks, dim):
    shape = list(blocks.shape[1:])
    shape[dim] *= blocks.shape[0]
    return jnp.moveaxis(blocks, 0, dim).reshape(shape)


def all_blocks(shard, axes, turns):
    blocks = shard[None]
    for k in turns:
        blocks = lax.all_gather(blocks, axes[k], axis=0, tiled=True)
    carried = [lax.axis_size(axes[k]) for k in reversed(turns)]
    blocks = blocks.reshape(*carried, *shard.shape)
    turned = sorted(range(len(turns)), key=lambda place: turns[len(turns) - 1 - place])
    return blocks.transpose(*turned, *range(len(turns), blocks.ndim)).reshape(-1, *shard.shape)


def whole_of(shard, axes, turns, dim):
    return in_order(all_blocks(shard, axes, turns), dim)


def copy_for_each(shard, axis):
    devices = lax.axis_size(axis)
    return lax.all_to_all(
        jnp.broadcast_to(shard[None], (devices, *shard.shape)), axis, 0, 0, tiled=True
    )


def gather_directly(shard, axis, dim):
    blocks = copy_for_each(shard, axis)
    return in_order(blocks, dim)


def rms_scale(source, scaling):
    floats = source.astype(jnp.float32)
    inverse = lax.rsqrt(jnp.mean(floats * floats, axis=-1, keepdims=True) + norm_eps)
    return (floats * inverse * scaling).astype(jnp.bfloat16)


def stick_block(queries, packed, shifting, carried, allowed):
    length, head_count, head_width = queries.shape
    key_part = packed[:, : head_count * head_width].reshape(length, head_count, head_width)
    value_part = packed[:, head_count * head_width :].reshape(length, head_count, head_width)
    scores = jnp.einsum("thd,shd->hts", queries, key_part, preferred_element_type=jnp.float32)
    scores = scores * head_width ** (-0.5) + shifting[:, None, :]
    log_stay = jnp.where(allowed, jax.nn.log_sigmoid(-scores), 0.0)
    between = lax.cumsum(log_stay, axis=2, reverse=True) - log_stay
    weights = jnp.where(
        allowed, jnp.exp(jax.nn.log_sigmoid(scores) + between + carried[:, :, None]), 0.0
    )
    contrib = jnp.einsum(
        "hts,shd->thd", weights.astype(jnp.bfloat16), value_part, preferred_element_type=jnp.float32
    )
    return (contrib, carried + jnp.sum(log_stay, axis=2))


def per_device(
    mixer_rows,
    mixer_gain,
    w_query,
    w_key,
    w_value,
    key_shift,
    w_out,
    expert_rows,
    expert_gain,
    routes,
    route_weight,
    w_gate,
    w_up,
    w_down,
):
    length = mixer_rows.shape[0]
    head_count = key_shift.shape[0]
    head_width = w_query.shape[1] // head_count
    normed = rms_scale(mixer_rows, mixer_gain)
    queries = jnp.dot(normed, w_query, preferred_element_type=jnp.float32).astype(jnp.bfloat16)
    key_rows = jnp.dot(normed, w_key, preferred_element_type=jnp.float32).astype(jnp.bfloat16)
    value_rows = jnp.dot(normed, w_value, preferred_element_type=jnp.float32).astype(jnp.bfloat16)
    queries = queries.reshape(length, head_count, head_width)
    packed = jnp.concatenate([key_rows, value_rows], axis=1)
    device = lax.axis_index(EP)
    positions = jnp.arange(length, dtype=jnp.int32)
    strict = (positions[None, :] < positions[:, None])[None]
    own_shift = lax.dynamic_slice_in_dim(key_shift, device * length, length, 1)
    summed, carried = stick_block(
        queries, packed, own_shift, jnp.zeros((head_count, length), jnp.float32), strict
    )
    gathered = whole_of(packed, EP, (0, 1), 0)

    def visiting(offset, status):
        running, carry_now = status
        anchor = device - offset
        block_rows = lax.dynamic_slice_in_dim(gathered, anchor * length, length, 0)
        shifting = lax.dynamic_slice_in_dim(key_shift, anchor * length, length, 1)
        contrib, carry_now = stick_block(queries, block_rows, shifting, carry_now, True)
        return (running + contrib, carry_now)

    summed, carried = lax.fori_loop(1, device + 1, visiting, (summed, carried))
    head_out = summed.reshape(length, head_count * head_width).astype(jnp.bfloat16)
    weight_rows = w_out
    mixer_out = jnp.dot(
        gather_directly(head_out, "tp", 1), weight_rows, preferred_element_type=jnp.float32
    ).astype(jnp.bfloat16)
    tokens_here, top_count = routes.shape
    expert_count = lax.axis_size(EP)
    capacity = 2 * tokens_here * top_count // expert_count
    rows_after_norm = rms_scale(expert_rows, expert_gain)
    chosen = routes.reshape(-1)
    hit_table = (chosen[:, None] == jnp.arange(expert_count, dtype=jnp.int32)[None, :]).astype(
        jnp.int32
    )
    places = jnp.sum((jnp.cumsum(hit_table, axis=0) - 1) * hit_table, axis=1)
    targets = chosen * capacity + places
    assign_ids = jnp.arange(tokens_here * top_count, dtype=jnp.int32) // top_count
    owners = (
        jnp.full((expert_count * capacity,), tokens_here, jnp.int32).at[targets].set(assign_ids)
    )
    padded = jnp.concatenate(
        [rows_after_norm, jnp.zeros((1, rows_after_norm.shape[1]), jnp.bfloat16)], axis=0
    )
    outgoing = padded[owners].reshape(expert_count, capacity, rows_after_norm.shape[1])
    gate_cols = w_gate[0]
    upper_cols = w_up[0]
    down_rows = w_down[0]
    portion_size = capacity // lax.axis_size("tp")
    own_slots = lax.dynamic_slice_in_dim(
        outgoing, lax.axis_index("tp") * portion_size, portion_size, 1
    )
    arrived = lax.all_to_all(own_slots, EP, split_axis=0, concat_axis=0, tiled=True)
    expert_arrived = lax.all_gather(arrived, "tp", axis=1, tiled=True)
    expert_senders, slots_here, feature_count = expert_arrived.shape
    flat_rows = expert_arrived.reshape(expert_senders * slots_here, feature_count)
    gating = jnp.minimum(
        jnp.dot(flat_rows, gate_cols, preferred_element_type=jnp.float32), glu_limit
    )
    linear = jnp.clip(
        jnp.dot(flat_rows, upper_cols, preferred_element_type=jnp.float32), -glu_limit, glu_limit
    )
    hidden = gating * jax.nn.sigmoid(glu_alpha * gating) * (linear + 1.0)
    hidden = hidden.astype(jnp.bfloat16).reshape(expert_senders, slots_here, gate_cols.shape[1])
    senders = hidden.shape[0]
    slot_total = hidden.shape[1]
    portion_units = lax.all_gather(hidden, "tp", axis=2, tiled=True)
    weight_rows = down_rows
    flat_units = portion_units.reshape(senders * slot_total, portion_units.shape[2])
    results = jnp.dot(flat_units, weight_rows, preferred_element_type=jnp.float32)
    leaving = results.astype(jnp.bfloat16).reshape(senders, slot_total, down_rows.shape[1])
    returned = lax.all_to_all(leaving, EP, split_axis=0, concat_axis=0, tiled=True)
    picked = returned.reshape(expert_count * capacity, down_rows.shape[1])[targets].astype(
        jnp.float32
    )
    picked = picked * route_weight.reshape(-1)[:, None]
    expert_out = jnp.sum(picked.reshape(tokens_here, top_count, down_rows.shape[1]), axis=1).astype(
        jnp.bfloat16
    )
    return (mixer_out, expert_out)


def solution(mesh):
    torus = Mesh(mesh.devices.reshape(16, 2, mesh.shape["tp"]), ("ep_0", "ep_1", "tp"))
    return jax.shard_map(
        per_device,
        mesh=torus,
        in_specs=(
            P(EP, None),
            P(),
            P(None, "tp"),
            P(None, "tp"),
            P(None, "tp"),
            P("tp", None),
            P(None, "tp"),
            P(EP, None),
            P(),
            P(EP, None),
            P(EP, None),
            P(EP, None, "tp"),
            P(EP, None, "tp"),
            P(EP, None, "tp"),
        ),
        out_specs=(P(EP, "tp"), P(EP, "tp")),
        check_vma=False,
    )
```

profile of v0, /device:TPU:1, one launch (start us, length us, event | category | flops | bytes accessed | tf_op | source)
XLA Modules:
  0.0 366.4 jit_solution(1222065985565656454)
XLA Ops:
  7.3 1.6 fusion.17
  8.9 1.8 convolution_convert_fusion.2
  12.5 1.2 reduce-window.26
  14.6 2.4 scatter_custom_fusion
  17.1 6.0 %gather_fusion = bf16[1024,2048]{1,0:T(8,128)(2,1)} fusion(bf16[129,2048]{1,0:T(8,128)(2,1)S(1)} %concatenate.7, s32[1024]{0:T(1024)S(1)} %fusion.44), kind=kCustom, calls=%fused_computation | custom fusion | bytes 8392704 | tf_op jit(solution)/shard_map/gather | solution.py:133
  23.1 1.5 constant_dynamic-slice_fusion.1
  24.6 40.3 %all_to_all.15 = bf16[32,2,2048]{2,1,0:T(2,128)(2,1)S(1)} all-to-all(bf16[32,2,2048]{2,1,0:T(2,128)(2,1)S(1)} %constant_dynamic-slice_fusion.1), channel_id=1, replica_groups=mesh['ep_0'=16,'ep_1'=2,'tp'=16] {'ep_0','ep_1'}, dimensions={0} | all-to-all | bytes 524288 | tf_op jit(solution)/shard_map/all_to_all | solution.py:141
  65.8 19.3 %all-gather.12.cloned.1.call-done = bf16[4096,128]{0,1:T(8,128)(2,1)} async-done(((bf16[256,128]{0,1:T(8,128)(2,1)}), bf16[4096,128]{0,1:T(8,128)(2,1)}) %all-gather.12.cloned.1.call-update) | async-done | bytes 1048592 | tf_op jit(solution)/shard_map/all_gather | solution.py:22
  85.1 2.5 copy.70
  87.8 72.1 %all-gather.8.cloned.1.call-done = bf16[32,32,2048]{2,0,1:T(8,128)(2,1)} async-done(((bf16[32,2,2048]{2,0,1:T(8,128)(2,1)}), bf16[32,32,2048]{2,0,1:T(8,128)(2,1)}) %all-gather.8.cloned.1.call-update) | async-done | bytes 4194320 | tf_op jit(solution)/shard_map/all_gather | solution.py:142
  159.9 4.5 %copy.67 = bf16[32,32,2048]{2,1,0:T(8,128)(2,1)S(1)} copy(bf16[32,32,2048]{2,0,1:T(8,128)(2,1)} %all-gather.8.cloned.1.call-done) | data formatting | bytes 8388608 | tf_op jit(solution)/shard_map/all_gather | solution.py:142
  164.4 1.3 convolution_minimum_fusion
  165.7 2.0 fusion.22
  169.3 2.3 fusion.39
  172.1 12.4 %all-gather.6.cloned.1.call-done = bf16[32,256,128]{1,0,2:T(8,128)(2,1)} async-done(((bf16[16,256,128]{1,0,2:T(8,128)(2,1)}), bf16[32,256,128]{1,0,2:T(8,128)(2,1)}) %all-gather.6.cloned.1.call-update) | async-done | bytes 2097168 | tf_op jit(solution)/shard_map/all_gather | solution.py:22
  184.5 3.5 copy.61
  187.9 4.1 %while.12 = (s32[]{:T(128)}, f32[256,1,64]{0,2,1:T(8,128)S(1)}, f32[1,256]{1,0:T(1,128)S(1)}, s32[]{:T(128)}, s32[]{:T(128)}, /*index=5*/bf16[8192,128]{1,0:T(8,...) while((s32[]{:T(128)}, f32[256,1,64]{0,2,1:T(8,128)S(1)}, ...), condition=%wide.region_8.9_spmd, body=%wide.region_4.8_spmd.sunk | while | flops 27083784 | bytes 2680031 | solution.py:110
  189.0 2.3 fusion.78
  192.9 5.5 %all-to-all-start = ((bf16[16,256,64]{1,2,0:T(8,128)(2,1)}), bf16[16,256,64]{1,2,0:T(8,128)(2,1)S(1)}, u32[]{:S(2)}, u32[]{:S(2)}) async-start(bf16[16,256,64]{1,2,0:T(8,128)(2,1)} %broadcast_in_dim.17), calls=%async_computation | async-start | bytes 1048576 | tf_op jit(solution)/shard_map/all_to_all | solution.py:35
  198.4 59.6 %all-gather.10.cloned.1.call-done = bf16[32,32,2048]{2,1,0:T(8,128)(2,1)} async-done(((bf16[32,32,128]{2,1,0:T(8,128)(2,1)}), bf16[32,32,2048]{2,1,0:T(8,128)(2,1)}) %all-gather.10.cloned.1.call-update) | async-done | bytes 4194320 | tf_op jit(solution)/shard_map/all_gather | solution.py:155
  258.0 4.3 %convolution_convert_fusion = bf16[1024,128]{1,0:T(8,128)(2,1)} fusion(bf16[1024,2048]{1,0:T(8,128)(2,1)} %bitcast.152, bf16[1,2048,128]{2,1,0:T(8,128)(2,1)} %param.29), kind=kOutput, calls=%fused_computation.40 | convolution fusion | flops 537001984 | bytes 4980736 | tf_op jit(solution)/shard_map/dot_general | solution.py:158
  262.3 73.1 %all-to-all-start.2 = ((bf16[32,32,128]{2,1,0:T(8,128)(2,1)}), bf16[32,32,128]{2,1,0:T(8,128)(2,1)S(1)}, u32[]{:S(2)}, u32[]{:S(2)}) async-start(bf16[32,32,128]{2,1,0:T(8,128)(2,1)} %bitcast.38), calls=%async_computation.2 | async-start | bytes 524288 | tf_op jit(solution)/shard_map/all_to_all | solution.py:160
  336.5 21.1 %all-to-all-done.2 = bf16[32,32,128]{2,1,0:T(8,128)(2,1)S(1)} async-done(((bf16[32,32,128]{2,1,0:T(8,128)(2,1)}), bf16[32,32,128]{2,1,0:T(8,128)(2,1)S(1)}, u32[]{:S(2)}, u32[]{:S(2)}) %all-to-all-start.2) | async-done | bytes 262176 | tf_op jit(solution)/shard_map/all_to_all | solution.py:160
  357.6 1.3 gather_fusion.1
  (78 shorter events, 10.4 us)
Async XLA Ops:
  7.2 157.2 %copy-start = (bf16[1,2048,128]{2,1,0:T(8,128)(2,1)S(1)}, bf16[1,2048,128]{2,1,0:T(8,128)(2,1)}, u32[]{:S(2)}) copy-start(bf16[1,2048,128]{2,1,0:T(8,128)(2,1)} %param.27) | copy-start | bytes 1572868
  7.2 3.6 copy-start.2
  7.2 3.6 copy-start.10
  7.2 3.6 copy-start.8
  7.2 77.9 %all-gather.12.cloned.1.call-start = ((), (), s32[]{:S(2)}) async-start(), calls=%async_computation.6 | async-start | bytes 1114112 | tf_op jit(solution)/shard_map/all_gather | solution.py:22
  8.9 3.1 copy-start.5
  8.9 3.4 copy-start.1
  10.8 2.9 copy-start.4
  12.0 147.9 %all-gather.8.cloned.1.call-start = ((), (), s32[]{:S(2)}) async-start(), calls=%async_computation.4 | async-start | bytes 4456448 | tf_op jit(solution)/shard_map/all_gather | solution.py:142
  65.8 118.7 %all-gather.6.cloned.1.call-start = ((), (), s32[]{:S(2)}) async-start(), calls=%async_computation.3 | async-start | bytes 3145728 | tf_op jit(solution)/shard_map/all_gather | solution.py:22
  87.6 170.4 %all-gather.10.cloned.1.call-start = ((), (), s32[]{:S(2)}) async-start(), calls=%async_computation.5 | async-start | bytes 4456448 | tf_op jit(solution)/shard_map/all_gather | solution.py:155
  164.4 1.3 copy-start.7
  165.7 2.7 copy-start.9
  192.9 69.4 %all-to-all-start = ((bf16[16,256,64]{1,2,0:T(8,128)(2,1)}), bf16[16,256,64]{1,2,0:T(8,128)(2,1)S(1)}, u32[]{:S(2)}, u32[]{:S(2)}) async-start(bf16[16,256,64]{1,2,0:T(8,128)(2,1)} %broadcast_in_dim.17), calls=%async_computation | async-start | bytes 1048576 | tf_op jit(solution)/shard_map/all_to_all | solution.py:35
  258.0 77.4 %copy-start.6 = (f32[128,4]{0,1:T(4,128)S(1)}, f32[128,4]{0,1:T(4,128)}, u32[]{:S(2)}) copy-start(f32[128,4]{0,1:T(4,128)} %param.26) | copy-start | bytes 6148
  258.0 77.5 %copy-start.3 = (bf16[1024,128]{1,0:T(8,128)(2,1)S(1)}, bf16[1024,128]{1,0:T(8,128)(2,1)}, u32[]{:S(2)}) copy-start(bf16[1024,128]{1,0:T(8,128)(2,1)} %param.22) | copy-start | bytes 786436
  262.3 95.3 %all-to-all-start.2 = ((bf16[32,32,128]{2,1,0:T(8,128)(2,1)}), bf16[32,32,128]{2,1,0:T(8,128)(2,1)S(1)}, u32[]{:S(2)}, u32[]{:S(2)}) async-start(bf16[32,32,128]{2,1,0:T(8,128)(2,1)} %bitcast.38), calls=%async_computation.2 | async-start | bytes 524288 | tf_op jit(solution)/shard_map/all_to_all | solution.py:160
Sparse Core Ops, SparseCore 0:
  12.1 72.9 all-gather.11
  88.1 71.7 all-gather.7
  162.0 22.4 all-gather.5
  187.3 70.6 all-gather.9
where the time goes:
time: 367 us; the launch traced here: 366 us
  waiting for transfers between devices  185 us (50%)
  starting transfers between devices  79 us (22%)
  blocking collectives  40.3 us (11%)
  local copies, waits for them, and re-layouts  25.8 us (7%)
  between operations  14.1 us (4%)
  matrix products  12.4 us (3%)
  other arithmetic  10.2 us (3%)
    all_to_all x1, starting transfers between devices, per_device(): lax.all_to_all(leaving, EP, split_axis=0, concat_axis=0, tiled=True)  73.1 us
    all_gather x1, waiting for transfers between devices, per_device(): expert_arrived = lax.all_gather(arrived, 'tp', axis=1, tiled=True)  72.1 us
    all_gather x1, waiting for transfers between devices, per_device(): portion_units = lax.all_gather(hidden, 'tp', axis=2, tiled=True)  59.6 us
    all_to_all x1, blocking collectives, per_device(): lax.all_to_all(own_slots, EP, split_axis=0, concat_axis=0, tiled=True)  40.3 us
    all_gather x2, waiting for transfers between devices, all_blocks(): blocks = lax.all_gather(blocks, axes[k], axis=0, tiled=True)  31.7 us
    all_to_all x1, waiting for transfers between devices, per_device(): lax.all_to_all(leaving, EP, split_axis=0, concat_axis=0, tiled=True)  21.1 us
  transfers between devices with their start and end apart: 6, of which 5 were waited for; matrix products, arithmetic and copies ran while one was open for 11% of the time, Pallas kernels for 0%

commit v1 on v0

--- a/solution.py
+++ b/solution.py
@@ -139,7 +139,9 @@
         outgoing, lax.axis_index("tp") * portion_size, portion_size, 1
     )
     arrived = lax.all_to_all(own_slots, EP, split_axis=0, concat_axis=0, tiled=True)
-    expert_arrived = lax.all_gather(arrived, "tp", axis=1, tiled=True)
+    expert_arrived = jnp.concatenate(
+        lax.all_to_all(jnp.stack([arrived] * lax.axis_size("tp")), "tp", 0, 0), axis=1
+    )
     expert_senders, slots_here, feature_count = expert_arrived.shape
     flat_rows = expert_arrived.reshape(expert_senders * slots_here, feature_count)
     gating = jnp.minimum(

time: 367 us -> 352 us (0.959)
  blocking collectives: 40.3 us -> 0 us
  starting transfers between devices: 79 us -> 107 us
  waiting for transfers between devices: 185 us -> 160 us
  local copies, waits for them, and re-layouts: 25.8 us -> 43.6 us
    all_gather x1 -> x0, waiting for transfers between devices: 72.1 us -> none  [per_device(): expert_arrived = lax.all_gather(arrived, 'tp', axis=1, tiled=True)]
    all_to_all x1 -> x0, blocking collectives: 40.3 us -> none  [per_device(): lax.all_to_all(own_slots, EP, split_axis=0, concat_axis=0, tiled=True)]
    all_gather x2, waiting for transfers between devices: 31.7 us -> 55.9 us  [all_blocks(): blocks = lax.all_gather(blocks, axes[k], axis=0, tiled=True)]
    all_to_all x0 -> x2, starting transfers between devices: none -> 23.7 us  [the longest x1 16.7 us: per_device(): lax.all_to_all(own_slots, EP, split_axis=0, concat_axis=0, tiled=True)]
    all_to_all x0 -> x2, waiting for transfers between devices: none -> 23.6 us  [the longest x1 22 us: per_device(): lax.all_to_all(own_slots, EP, split_axis=0, concat_axis=0, tiled=True)]
    another operation x8 -> x10, local copies, waits for them, and re-layouts: 0.28 us -> 13 us  [the longest x1 7.21 us: per_device(): expert_arrived.reshape(expert_senders * slots_here, feature_count)]
    reshape x0 -> x1, local copies, waits for them, and re-layouts: none -> 8.69 us  [per_device(): jnp.concatenate(lax.all_to_all(jnp.stack([arrived] * lax.axis_size('tp'))...]
    all_to_all x1, starting transfers between devices: 73.1 us -> 77.9 us  [per_device(): lax.all_to_all(leaving, EP, split_axis=0, concat_axis=0, tiled=True)]
  transfers between devices with their start and end apart: 6 -> 7, of which waited for: 5 -> 5; matrix products, arithmetic and copies ran while one was open for 11% -> 13% of each run, Pallas kernels for 0% -> 0%
where the time goes in v1:
time: 352 us; the launch traced here: 350 us
  waiting for transfers between devices  160 us (45%)
  starting transfers between devices  107 us (30%)
  local copies, waits for them, and re-layouts  43.6 us (12%)
  between operations  14 us (4%)
  matrix products  13.4 us (4%)
  other arithmetic  11.6 us (3%)
    all_to_all x1, starting transfers between devices, per_device(): lax.all_to_all(leaving, EP, split_axis=0, concat_axis=0, tiled=True)  77.9 us
    all_gather x1, waiting for transfers between devices, per_device(): portion_units = lax.all_gather(hidden, 'tp', axis=2, tiled=True)  59.5 us
    all_gather x2, waiting for transfers between devices, all_blocks(): blocks = lax.all_gather(blocks, axes[k], axis=0, tiled=True)  55.9 us
    all_to_all x1, waiting for transfers between devices, per_device(): lax.all_to_all(own_slots, EP, split_axis=0, concat_axis=0, tiled=True)  22 us
    all_to_all x1, waiting for transfers between devices, per_device(): lax.all_to_all(leaving, EP, split_axis=0, concat_axis=0, tiled=True)  21.1 us
    all_to_all x1, starting transfers between devices, per_device(): lax.all_to_all(own_slots, EP, split_axis=0, concat_axis=0, tiled=True)  16.7 us
    reshape x1, local copies, waits for them, and re-layouts, per_device(): jnp.concatenate(lax.all_to_all(jnp.stack([arrived] * lax.axis_size('tp'))...  8.69 us
    another operation x1, local copies, waits for them, and re-layouts, per_device(): expert_arrived.reshape(expert_senders * slots_here, feature_count)  7.21 us
  transfers between devices with their start and end apart: 7, of which 5 were waited for; matrix products, arithmetic and copies ran while one was open for 13% of the time, Pallas kernels for 0%

profile of v1, /device:TPU:1, one launch (start us, length us, event | category | flops | bytes accessed | tf_op | source)
XLA Modules:
  0.0 350.4 jit_solution(3256165288962291582)
XLA Ops:
  10.7 2.4 scatter_custom_fusion
  15.7 6.0 %gather_fusion = bf16[1024,2048]{1,0:T(8,128)(2,1)} fusion(bf16[129,2048]{1,0:T(8,128)(2,1)S(1)} %concatenate.7, s32[1024]{0:T(1024)S(1)} %fusion.44), kind=kCustom, calls=%fused_computation | custom fusion | bytes 8392704 | tf_op jit(solution)/shard_map/gather | solution.py:133
  21.8 2.2 constant_dynamic-slice_fusion.1
  23.9 16.7 %all-to-all-start.1 = ((bf16[32,2,2048]{2,1,0:T(2,128)(2,1)}), bf16[32,2,2048]{2,1,0:T(2,128)(2,1)S(1)}, u32[]{:S(2)}, u32[]{:S(2)}) async-start(bf16[32,2,2048]{2,1,0:T(2,128)(2,1)} %constant_dynamic-slice_fusion.1), calls=%async_computation.1 | async-start | bytes 524288 | tf_op jit(solution)/shard_map/all_to_all | solution.py:141
  41.0 22.0 %all-to-all-done.1 = bf16[32,2,2048]{2,1,0:T(2,128)(2,1)S(1)} async-done(((bf16[32,2,2048]{2,1,0:T(2,128)(2,1)}), bf16[32,2,2048]{2,1,0:T(2,128)(2,1)S(1)}, u32[]{:S(2)}, u32[]{:S(2)}) %all-to-all-start.1) | async-done | bytes 262176 | tf_op jit(solution)/shard_map/all_to_all | solution.py:141
  62.9 5.5 %stack.2 = bf16[16,32,2,2048]{3,2,1,0:T(2,128)(2,1)} broadcast(bf16[32,2,2048]{2,1,0:T(2,128)(2,1)S(1)} %all-to-all-done.1), dimensions={1,2,3} | broadcast | bytes 4456448 | tf_op jit(solution)/shard_map/stack | solution.py:143
  68.4 6.9 %all-to-all-start.2 = ((bf16[16,32,2,2048]{3,2,1,0:T(2,128)(2,1)}), bf16[16,32,2,2048]{3,2,1,0:T(2,128)(2,1)}, u32[]{:S(2)}, u32[]{:S(2)}) async-start(bf16[16,32,2,2048]{3,2,1,0:T(2,128)(2,1)} %stack.2), calls=%async_computation.2 | async-start | bytes 8388608 | tf_op jit(solution)/shard_map/all_to_all | solution.py:143
  77.5 55.9 %all-gather.9.cloned.1.call-done = bf16[4096,128]{0,1:T(8,128)(2,1)} async-done(((bf16[256,128]{0,1:T(8,128)(2,1)}), bf16[4096,128]{0,1:T(8,128)(2,1)}) %all-gather.9.cloned.1.call-update) | async-done | bytes 1048592 | tf_op jit(solution)/shard_map/all_gather | solution.py:22
  133.5 2.5 copy.46
  136.2 1.7 all-to-all-done.2
  137.9 8.7 %copy.43 = bf16[32,16,2,2048]{3,2,1,0:T(2,128)(2,1)} copy(bf16[32,16,2,2048]{3,2,0,1:T(2,128)(2,1)} %bitcast.32) | data formatting | bytes 8388608 | tf_op jit(solution)/shard_map/reshape | solution.py:142
  146.5 7.2 %reshape_reshape.7 = bf16[1024,2048]{1,0:T(8,128)(2,1)} reshape(bf16[32,16,2,2048]{3,2,1,0:T(2,128)(2,1)} %copy.43) | data formatting | bytes 8388608 | tf_op jit(solution)/shard_map/reshape;reshape | solution.py:146
  153.8 3.6 %convolution_minimum_fusion = f32[1024,128]{1,0:T(8,128)S(1)} fusion(bf16[1024,2048]{1,0:T(8,128)(2,1)} %reshape_reshape.7, bf16[1,2048,128]{2,1,0:T(8,128)(2,1)S(1)} %copy-done), kind=kOutput, calls=%fused_computation.36 | convolution fusion | flops 537001984 | bytes 5242880 | tf_op jit(solution)/shard_map/dot_general | solution.py:148
  157.4 2.0 fusion.22
  161.0 2.3 fusion.39
  163.8 3.5 copy.38
  167.3 4.3 %while.12 = (s32[]{:T(128)}, f32[256,1,64]{0,2,1:T(8,128)S(1)}, f32[1,256]{1,0:T(1,128)S(1)}, s32[]{:T(128)}, s32[]{:T(128)}, /*index=5*/bf16[8192,128]{1,0:T(8,...) while((s32[]{:T(128)}, f32[256,1,64]{0,2,1:T(8,128)S(1)}, ...), condition=%wide.region_8.9_spmd, body=%wide.region_4.8_spmd.sunk | while | flops 27083784 | bytes 2680031 | solution.py:110
  168.5 2.3 fusion.78
  172.4 5.3 %all-to-all-start = ((bf16[16,256,64]{1,2,0:T(8,128)(2,1)}), bf16[16,256,64]{1,2,0:T(8,128)(2,1)S(1)}, u32[]{:S(2)}, u32[]{:S(2)}) async-start(bf16[16,256,64]{1,2,0:T(8,128)(2,1)} %broadcast_in_dim.17), calls=%async_computation | async-start | bytes 1048576 | tf_op jit(solution)/shard_map/all_to_all | solution.py:35
  177.7 59.5 %all-gather.7.cloned.1.call-done = bf16[32,32,2048]{2,1,0:T(8,128)(2,1)} async-done(((bf16[32,32,128]{2,1,0:T(8,128)(2,1)}), bf16[32,32,2048]{2,1,0:T(8,128)(2,1)}) %all-gather.7.cloned.1.call-update) | async-done | bytes 4194320 | tf_op jit(solution)/shard_map/all_gather | solution.py:157
  237.2 4.3 %convolution_convert_fusion = bf16[1024,128]{1,0:T(8,128)(2,1)} fusion(bf16[1024,2048]{1,0:T(8,128)(2,1)} %bitcast.150, bf16[1,2048,128]{2,1,0:T(8,128)(2,1)} %param.29), kind=kOutput, calls=%fused_computation.40 | convolution fusion | flops 537001984 | bytes 4980736 | tf_op jit(solution)/shard_map/dot_general | solution.py:160
  241.5 77.9 %all-to-all-start.3 = ((bf16[32,32,128]{2,1,0:T(8,128)(2,1)}), bf16[32,32,128]{2,1,0:T(8,128)(2,1)S(1)}, u32[]{:S(2)}, u32[]{:S(2)}) async-start(bf16[32,32,128]{2,1,0:T(8,128)(2,1)} %bitcast.38), calls=%async_computation.3 | async-start | bytes 524288 | tf_op jit(solution)/shard_map/all_to_all | solution.py:162
  320.5 21.1 %all-to-all-done.3 = bf16[32,32,128]{2,1,0:T(8,128)(2,1)S(1)} async-done(((bf16[32,32,128]{2,1,0:T(8,128)(2,1)}), bf16[32,32,128]{2,1,0:T(8,128)(2,1)S(1)}, u32[]{:S(2)}, u32[]{:S(2)}) %all-to-all-start.3) | async-done | bytes 262176 | tf_op jit(solution)/shard_map/all_to_all | solution.py:162
  341.7 1.3 gather_fusion.1
  (77 shorter events, 15.3 us)
Async XLA Ops:
  7.2 146.6 %copy-start = (bf16[1,2048,128]{2,1,0:T(8,128)(2,1)S(1)}, bf16[1,2048,128]{2,1,0:T(8,128)(2,1)}, u32[]{:S(2)}) copy-start(bf16[1,2048,128]{2,1,0:T(8,128)(2,1)} %param.27) | copy-start | bytes 1572868
  15.7 25.0 %copy-start.2 = (bf16[256,2048]{1,0:T(8,128)(2,1)S(1)}, bf16[256,2048]{1,0:T(8,128)(2,1)}, u32[]{:S(2)}) copy-start(bf16[256,2048]{1,0:T(8,128)(2,1)} %param.16) | copy-start | bytes 3145732
  23.9 39.0 %all-to-all-start.1 = ((bf16[32,2,2048]{2,1,0:T(2,128)(2,1)}), bf16[32,2,2048]{2,1,0:T(2,128)(2,1)S(1)}, u32[]{:S(2)}, u32[]{:S(2)}) async-start(bf16[32,2,2048]{2,1,0:T(2,128)(2,1)} %constant_dynamic-slice_fusion.1), calls=%async_computation.1 | async-start | bytes 524288 | tf_op jit(solution)/shard_map/all_to_all | solution.py:141
  68.4 7.0 %copy-start.6 = (bf16[2048,64]{0,1:T(8,128)(2,1)S(1)}, bf16[2048,64]{0,1:T(8,128)(2,1)}, u32[]{:S(2)}) copy-start(bf16[2048,64]{0,1:T(8,128)(2,1)} %param.19) | copy-start | bytes 786436
  68.4 7.0 %copy-start.9 = (f32[2048]{0:T(1024)S(1)}, f32[2048]{0:T(1024)}, u32[]{:S(2)}) copy-start(f32[2048]{0:T(1024)} %param.17) | copy-start | bytes 24580
  68.4 69.4 %all-to-all-start.2 = ((bf16[16,32,2,2048]{3,2,1,0:T(2,128)(2,1)}), bf16[16,32,2,2048]{3,2,1,0:T(2,128)(2,1)}, u32[]{:S(2)}, u32[]{:S(2)}) async-start(bf16[16,32,2,2048]{3,2,1,0:T(2,128)(2,1)} %stack.2), calls=%async_computation.2 | async-start | bytes 8388608 | tf_op jit(solution)/shard_map/all_to_all | solution.py:143
  75.4 1.0 copy-start.7
  75.4 58.1 %all-gather.9.cloned.1.call-start = ((), (), s32[]{:S(2)}) async-start(), calls=%async_computation.6 | async-start | bytes 1114112 | tf_op jit(solution)/shard_map/all_gather | solution.py:22
  77.5 86.3 %all-gather.5.cloned.1.call-start = ((), (), s32[]{:S(2)}) async-start(), calls=%async_computation.4 | async-start | bytes 3145728 | tf_op jit(solution)/shard_map/all_gather | solution.py:22
  136.0 101.2 %all-gather.7.cloned.1.call-start = ((), (), s32[]{:S(2)}) async-start(), calls=%async_computation.5 | async-start | bytes 4456448 | tf_op jit(solution)/shard_map/all_gather | solution.py:157
  153.8 3.6 %copy-start.1 = (bf16[1024,2048]{1,0:T(8,128)(2,1)S(1)}, bf16[1024,2048]{1,0:T(8,128)(2,1)}, u32[]{:S(2)}) copy-start(bf16[1024,2048]{1,0:T(8,128)(2,1)} %reshape_reshape.7) | copy-start | bytes 12582916
  153.8 3.6 %copy-start.5 = (bf16[1,2048,128]{2,1,0:T(8,128)(2,1)S(1)}, bf16[1,2048,128]{2,1,0:T(8,128)(2,1)}, u32[]{:S(2)}) copy-start(bf16[1,2048,128]{2,1,0:T(8,128)(2,1)} %param.28) | copy-start | bytes 1572868
  157.4 2.7 copy-start.8
  172.4 69.1 %all-to-all-start = ((bf16[16,256,64]{1,2,0:T(8,128)(2,1)}), bf16[16,256,64]{1,2,0:T(8,128)(2,1)S(1)}, u32[]{:S(2)}, u32[]{:S(2)}) async-start(bf16[16,256,64]{1,2,0:T(8,128)(2,1)} %broadcast_in_dim.17), calls=%async_computation | async-start | bytes 1048576 | tf_op jit(solution)/shard_map/all_to_all | solution.py:35
  237.2 82.2 %copy-start.4 = (f32[128,4]{0,1:T(4,128)S(1)}, f32[128,4]{0,1:T(4,128)}, u32[]{:S(2)}) copy-start(f32[128,4]{0,1:T(4,128)} %param.26) | copy-start | bytes 6148
  237.2 82.3 %copy-start.3 = (bf16[1024,128]{1,0:T(8,128)(2,1)S(1)}, bf16[1024,128]{1,0:T(8,128)(2,1)}, u32[]{:S(2)}) copy-start(bf16[1024,128]{1,0:T(8,128)(2,1)} %param.22) | copy-start | bytes 786436
  241.5 100.1 %all-to-all-start.3 = ((bf16[32,32,128]{2,1,0:T(8,128)(2,1)}), bf16[32,32,128]{2,1,0:T(8,128)(2,1)S(1)}, u32[]{:S(2)}, u32[]{:S(2)}) async-start(bf16[32,32,128]{2,1,0:T(8,128)(2,1)} %bitcast.38), calls=%async_computation.3 | async-start | bytes 524288 | tf_op jit(solution)/shard_map/all_to_all | solution.py:162
Sparse Core Ops, SparseCore 0:
  78.8 54.6 all-gather.8
  136.1 27.3 all-gather.4
  166.5 70.6 all-gather.6
